TPU v7x, 32 devices: a whole 2x2x4 slice. The times are simulated.
32 devices in a mesh: sp: 8 (over z, x), tp: 4 (over y, core).
Axes of the slice: x: 2, y: 2, z: 4, core: 2. Of those that a mesh axis runs over, the one named last changes fastest.
Arguments:
- saved_tokens: bfloat16 [1536, 2048], P('sp'), may hold values from -3.75 to 3.75
- cotangent: bfloat16 [1536, 2048], P('sp'), may hold values from -6 to 6
- routes: int32 [1536, 2], P('sp'), may hold values from 0 to 7, all different within a row; in each aligned block of 192 rows (0 to 191, 192 to 383, ...) at most 96 rows name the same one
- route_weights: float32 [1536, 2], P('sp'), may hold values from 0.2 to 1
- gate_in: bfloat16 [1536, 1024], P('sp', 'tp'), may hold values from -6 to 6
- conv_in: bfloat16 [1536, 1024], P('sp', 'tp'), may hold values from -6 to 6
- value_in: bfloat16 [1536, 1024], P('sp', 'tp'), may hold values from -6 to 6
- conv_taps: float32 [3, 1024], replicated, may hold values from -3.5 to 3.5
- out_weight: bfloat16 [2048, 1024], P(None, 'tp'), may hold values from -0.1875 to 0.1875
- gate_proj: bfloat16 [8, 2048, 2048], P('sp', None, 'tp'), may hold values from -0.125 to 0.125
- up_proj: bfloat16 [8, 2048, 2048], P('sp', None, 'tp'), may hold values from -0.125 to 0.125
- down_proj: bfloat16 [8, 2048, 2048], P('sp', 'tp'), may hold values from -0.125 to 0.125
Outputs:
- gate_proj_grad: float32 [8, 2048, 2048], P('sp', None, 'tp')
- up_proj_grad: float32 [8, 2048, 2048], P('sp', None, 'tp')
- down_proj_grad: float32 [8, 2048, 2048], P('sp', 'tp')
- out_weight_grad: float32 [2048, 1024], P('sp', 'tp')
- token_grad: bfloat16 [1536, 2048], P('sp', 'tp')
- gate_in_grad: bfloat16 [1536, 1024], P('sp', 'tp')
- conv_in_grad: bfloat16 [1536, 1024], P('sp', 'tp')
- value_in_grad: bfloat16 [1536, 1024], P('sp', 'tp')
Inputs may be any that keep to these rules, and one draw needn't show every extreme that they name: `routes`: within each aligned block of 192 tokens at most 96 assignments name one expert, a bound that some block reaches of them; the 2 experts of a token differ.
All inputs are finite; a program needn't handle non-finite values.
Results may differ from a plain program's by a relative error of at most 0.0063.
Values may be sent and summed in bfloat16 or wider, within the bound.
A program may use at most 64 MiB of HBM per device.

v0:
```python
import jax
import jax.numpy as jnp
from jax import lax
from jax.sharding import PartitionSpec as P

CLAMP_LIMIT = 7.0
SILU_ALPHA = 1.702


def padded(cells, sides, width):
    for axis, dim in sides:
        count = lax.axis_size(axis)
        ends = count - 1
        head = lax.slice_in_dim(cells, 0, width, axis=dim)
        tail = lax.slice_in_dim(cells, cells.shape[dim] - width, cells.shape[dim], axis=dim)
        cells = jnp.concatenate(
            [
                lax.ppermute(tail, axis, [(i, (i + 1) % count) for i in range(ends)]),
                cells,
                lax.ppermute(head, axis, [((i + 1) % count, i) for i in range(ends)]),
            ],
            axis=dim,
        )
    return cells


def contract_rows(left, right):
    return lax.dot_general(
        left, right, (((0,), (0,)), ((), ())), preferred_element_type=jnp.float32
    )


def contract_cols(left, right):
    return lax.dot_general(
        left, right, (((1,), (1,)), ((), ())), preferred_element_type=jnp.float32
    )


def expert_backward(rows_in, grads_in, w_gate, w_up, w_down):
    gate_pre = jnp.dot(rows_in, w_gate, preferred_element_type=jnp.float32)
    up_pre = jnp.dot(rows_in, w_up, preferred_element_type=jnp.float32)
    gate_clip = jnp.minimum(gate_pre, CLAMP_LIMIT)
    up_clip = jnp.clip(up_pre, -CLAMP_LIMIT, CLAMP_LIMIT)
    sigmoid_gate = jax.nn.sigmoid(SILU_ALPHA * gate_clip)
    gated_act = gate_clip * sigmoid_gate
    hidden = ((up_clip + 1.0) * gated_act).astype(jnp.bfloat16)
    d_hidden = contract_cols(grads_in, w_down)
    d_up = jnp.where(jnp.abs(up_pre) < CLAMP_LIMIT, d_hidden * gated_act, 0.0).astype(jnp.bfloat16)
    gate_slope = sigmoid_gate + SILU_ALPHA * gate_clip * sigmoid_gate * (1.0 - sigmoid_gate)
    d_gate = jnp.where(gate_pre < CLAMP_LIMIT, d_hidden * (up_clip + 1.0) * gate_slope, 0.0).astype(
        jnp.bfloat16
    )
    down_grad = contract_rows(hidden, grads_in)
    gate_grad = contract_rows(rows_in, d_gate)
    up_grad = contract_rows(rows_in, d_up)
    partial_value = contract_cols(d_gate, w_gate) + contract_cols(d_up, w_up)
    return (gate_grad, up_grad, down_grad, partial_value.astype(jnp.bfloat16))


def local(
    saved_tokens,
    cotangent,
    routes,
    route_weights,
    gate_in,
    conv_in,
    value_in,
    conv_taps,
    out_weight,
    gate_proj,
    up_proj,
    down_proj,
):
    tok_rows, model_width = saved_tokens.shape
    top_count = routes.shape[1]
    expert_count = lax.axis_size("sp")
    tp_count = lax.axis_size("tp")
    capacity = 2 * tok_rows * top_count // expert_count
    assigns = tok_rows * top_count
    part_width = model_width // tp_count
    offset = lax.axis_index("tp") * part_width
    flat_routes = routes.reshape(assigns)
    onehot = (flat_routes[:, None] == jnp.arange(expert_count, dtype=jnp.int32)[None, :]).astype(
        jnp.int32
    )
    slot_rank = jnp.sum((jnp.cumsum(onehot, axis=0) - 1) * onehot, axis=1)
    slot_index = flat_routes * capacity + slot_rank
    slot_owner = (
        jnp.full((expert_count * capacity,), assigns, jnp.int32)
        .at[slot_index]
        .set(jnp.arange(assigns, dtype=jnp.int32))
    )
    zero_row = jnp.zeros((1, model_width), jnp.bfloat16)
    token_rows = jnp.concatenate([saved_tokens, zero_row], 0)[slot_owner // top_count]
    scaled = (route_weights[:, :, None] * cotangent.astype(jnp.float32)[:, None, :]).astype(
        jnp.bfloat16
    )
    grad_rows = jnp.concatenate([scaled.reshape(assigns, model_width), zero_row], 0)[slot_owner]
    send_tokens = token_rows.reshape(expert_count, capacity, model_width)
    send_grads = grad_rows.reshape(expert_count, capacity, model_width)
    sliced = (
        lax.dynamic_slice_in_dim(send_tokens, offset, part_width, 2),
        lax.dynamic_slice_in_dim(send_grads, offset, part_width, 2),
    )
    arrived = (
        lax.all_to_all(sliced[0], "sp", split_axis=0, concat_axis=0, tiled=True),
        lax.all_to_all(sliced[1], "sp", split_axis=0, concat_axis=0, tiled=True),
    )
    recv_tokens, recv_grads = (
        lax.all_gather(arrived[0], "tp", axis=2, tiled=True),
        lax.all_gather(arrived[1], "tp", axis=2, tiled=True),
    )
    gate_grad, up_grad, down_grad, partial_value = expert_backward(
        recv_tokens.reshape(-1, model_width),
        recv_grads.reshape(-1, model_width),
        gate_proj[0],
        up_proj[0],
        down_proj[0],
    )
    grouped = partial_value.reshape(expert_count * capacity, tp_count, part_width)
    pieces = lax.all_to_all(grouped, "tp", split_axis=1, concat_axis=1, tiled=True)
    shares = jnp.sum(pieces.astype(jnp.float32), axis=1).reshape(expert_count, capacity, part_width)
    returned = lax.all_to_all(shares, "sp", split_axis=0, concat_axis=0, tiled=True)
    picked = returned.reshape(-1, part_width)[slot_index]
    combined = jnp.sum(picked.reshape(tok_rows, top_count, part_width), axis=1)
    own_cot = lax.dynamic_slice_in_dim(cotangent, offset, part_width, 1).astype(jnp.float32)
    token_grad = (own_cot + combined).astype(jnp.bfloat16)
    residual = lax.all_gather(token_grad, "tp", axis=1, tiled=True)
    channels = gate_in.shape[1]
    d_conv_out = jnp.dot(residual, out_weight, preferred_element_type=jnp.float32)
    gate_f32 = gate_in.astype(jnp.float32)
    conv_f32 = conv_in.astype(jnp.float32)
    value_f32 = value_in.astype(jnp.float32)
    product = conv_f32 * value_f32
    back_signal = d_conv_out * gate_f32
    rimmed = padded(jnp.concatenate([product, back_signal], 1), (("sp", 0),), 1)
    prod_rim = rimmed[:, :channels]
    grad_rim = rimmed[:, channels:]
    my_taps = lax.dynamic_slice_in_dim(conv_taps, lax.axis_index("tp") * channels, channels, 1)
    conv_out = my_taps[0] * prod_rim[:-2] + my_taps[1] * prod_rim[1:-1] + my_taps[2] * prod_rim[2:]
    d_product = my_taps[0] * grad_rim[2:] + my_taps[1] * grad_rim[1:-1] + my_taps[2] * grad_rim[:-2]
    gate_in_grad = (d_conv_out * conv_out).astype(jnp.bfloat16)
    conv_in_grad = (d_product * value_f32).astype(jnp.bfloat16)
    value_in_grad = (d_product * conv_f32).astype(jnp.bfloat16)
    mixed_act = (gate_f32 * conv_out).astype(jnp.bfloat16)
    out_weight_grad = lax.psum_scatter(
        contract_rows(residual, mixed_act), "sp", scatter_dimension=0, tiled=True
    )
    return (
        gate_grad[None],
        up_grad[None],
        down_grad[None],
        out_weight_grad,
        token_grad,
        gate_in_grad,
        conv_in_grad,
        value_in_grad,
    )


def solution(mesh):
    in_specs = (
        P("sp", None),
        P("sp", None),
        P("sp", None),
        P("sp", None),
        P("sp", "tp"),
        P("sp", "tp"),
        P("sp", "tp"),
        P(),
        P(None, "tp"),
        P("sp", None, "tp"),
        P("sp", None, "tp"),
        P("sp", "tp", None),
    )
    out_specs = (
        P("sp", None, "tp"),
        P("sp", None, "tp"),
        P("sp", "tp", None),
        P("sp", "tp"),
        P("sp", "tp"),
        P("sp", "tp"),
        P("sp", "tp"),
        P("sp", "tp"),
    )
    return jax.shard_map(local, mesh=mesh, in_specs=in_specs, out_specs=out_specs, check_vma=False)
```

profile of v0, /device:TPU:0, one launch (start us, length us, event | category | flops | bytes accessed | tf_op | source)
XLA Modules:
  0.0 314.1 jit_solution(3205792691582930578)
XLA Ops:
  10.7 2.9 scatter_custom_fusion
  13.6 1.2 concatenate.18
  14.8 4.2 %gather_fusion = bf16[768,2048]{1,0:T(8,128)(2,1)} fusion(bf16[193,2048]{1,0:T(8,128)(2,1)S(1)} %concatenate.18, s32[1024]{0:T(1024)S(1)} %get-tuple-element.22), kind=kCustom, calls=%fused_computation | custom fusion | bytes 6294528 | tf_op jit(solution)/shard_map/gather | solution.py:94
  19.1 1.3 constant_dynamic-slice_fusion.2
  20.3 27.3 %all_to_all.20 = bf16[8,96,512]{2,1,0:T(8,128)(2,1)} all-to-all(bf16[8,96,512]{2,1,0:T(8,128)(2,1)S(1)} %constant_dynamic-slice_fusion.2), channel_id=1, replica_groups=mesh['sp'=8,'tp'=4] {'sp'}, dimensions={0} | all-to-all | bytes 1572864 | tf_op jit(solution)/shard_map/all_to_all | solution.py:106
  47.7 3.3 %mul.141 = f32[192,2,2048]{2,1,0:T(2,128)} broadcast(bf16[192,2048]{1,0:T(8,128)(2,1)S(1)} %copy-done.3), dimensions={0,2} | broadcast | bytes 3932160 | tf_op jit(solution)/shard_map/mul | solution.py:95
  51.0 5.4 %mul.142 = f32[384,2048]{1,0:T(8,128)} reshape(f32[192,2,2048]{2,1,0:T(2,128)} %mul.141) | data formatting | bytes 6291456 | tf_op jit(solution)/shard_map/mul | solution.py:95
  56.7 2.1 multiply_convert_fusion
  58.8 1.3 concatenate.19
  60.1 8.7 %gather_fusion.1 = bf16[768,2048]{1,0:T(8,128)(2,1)} fusion(bf16[385,2048]{1,0:T(8,128)(2,1)} %concatenate.19, s32[1024]{0:T(1024)S(1)} %get-tuple-element.21), kind=kCustom, calls=%fused_computation.1 | custom fusion | bytes 6294528 | tf_op jit(solution)/shard_map/gather | solution.py:98
  68.8 1.2 constant_dynamic-slice_fusion.1
  70.0 23.4 %all_to_all.21 = bf16[8,96,512]{2,1,0:T(8,128)(2,1)} all-to-all(bf16[8,96,512]{2,1,0:T(8,128)(2,1)S(1)} %constant_dynamic-slice_fusion.1), channel_id=1, replica_groups=mesh['sp'=8,'tp'=4] {'sp'}, dimensions={0} | all-to-all | bytes 1572864 | tf_op jit(solution)/shard_map/all_to_all | solution.py:107
  93.5 5.6 %fusion.1 = f32[768,512]{1,0:T(8,128)} fusion(bf16[768,2048]{1,0:T(8,128)(2,1)} %bitcast.70, bf16[1,2048,512]{2,1,0:T(8,128)(2,1)} %param.22), kind=kOutput, calls=%fused_computation.12 | convolution fusion | flops 1610612736 | bytes 6815744 | tf_op jit(solution)/shard_map/dot_general | solution.py:41
  99.1 3.0 fusion.7
  102.1 19.1 %all-gather.5.cloned.1.call-done = bf16[8,96,2048]{2,1,0:T(8,128)(2,1)} async-done(((bf16[8,96,512]{2,1,0:T(8,128)(2,1)}), bf16[8,96,2048]{2,1,0:T(8,128)(2,1)}) %all-gather.5.cloned.1.call-update) | async-done | bytes 3145744 | tf_op jit(solution)/shard_map/all_gather | solution.py:111
  121.2 6.1 %select_convert_fusion = (bf16[768,512]{1,0:T(8,128)(2,1)S(1)}, bf16[768,512]{1,0:T(8,128)(2,1)S(1)}) fusion(f32[768,512]{1,0:T(8,128)} %fusion.1, f32[768,512]{1,0:T(8,128)} %fusion.7, bf16[768,2048]{1,0:T(8,128)(2,1)} %bitcast.74, bf16[1,512,2048]{2,1,0:T(8,128)(2,1)} %param.23), kind=kOutput, calls=%fused_computation.21 | convolution fusion | flops 1619263488 | bytes 9961472 | tf_op jit(solution)/shard_map/dot_general | solution.py:34
  127.4 1.8 fusion.5
  129.6 1.8 add_convert_fusion
  131.7 39.4 %all_to_all.22 = bf16[768,4,512]{2,0,1:T(8,128)(2,1)S(1)} all-to-all(bf16[768,4,512]{2,0,1:T(8,128)(2,1)S(1)} %bitcast.55), channel_id=1, replica_groups=mesh['sp'=8,'tp'=4] {'tp'}, dimensions={1} | all-to-all | bytes 6291456 | tf_op jit(solution)/shard_map/all_to_all | solution.py:121
  171.1 1.6 convert_reduce_fusion
  172.8 5.6 %all-to-all-start.3 = ((f32[8,96,512]{2,1,0:T(8,128)}), f32[8,96,512]{2,1,0:T(8,128)S(1)}, u32[]{:S(2)}, u32[]{:S(2)}) async-start(f32[8,96,512]{2,1,0:T(8,128)} %bitcast.57), calls=%async_computation.3 | async-start | bytes 3145728 | tf_op jit(solution)/shard_map/all_to_all | solution.py:123
  178.5 36.5 %all-to-all-done.3 = f32[8,96,512]{2,1,0:T(8,128)S(1)} async-done(((f32[8,96,512]{2,1,0:T(8,128)}), f32[8,96,512]{2,1,0:T(8,128)S(1)}, u32[]{:S(2)}, u32[]{:S(2)}) %all-to-all-start.3) | async-done | bytes 1572896 | tf_op jit(solution)/shard_map/all_to_all | solution.py:123
  215.1 1.6 gather_fusion.2
  219.8 7.9 %all_gather.11 = bf16[192,2048]{1,0:T(8,128)(2,1)S(1)} all-gather(bf16[192,512]{1,0:T(8,128)(2,1)S(1)} %add_convert_fusion.1), channel_id=1, replica_groups=mesh['sp'=8,'tp'=4] {'tp'}, dimensions={1}, use_global_device_ids=true | all-gather | bytes 983040 | tf_op jit(solution)/shard_map/all_gather | solution.py:128
  228.8 3.3 %collective-permute-start = (f32[1,512]{1,0:T(1,128)S(1)}, f32[1,512]{1,0:T(1,128)S(1)}, u32[]{:S(2)}, u32[]{:S(2)}) collective-permute-start(f32[1,512]{1,0:T(1,128)S(1)} %get-tuple-element.12), channel_id=1, source_target_pairs={{0,4},{4,8},{8,12},{12,16},{16,20},{20,24},{24,28},{1,5},{5,9},{9,... | collective-permute-start | bytes 6152 | tf_op jit(solution)/shard_map/ppermute | solution.py:18
  232.1 1.5 collective-permute-start.1
  234.5 3.1 collective-permute-done.1
  237.6 1.9 fusion.21
  239.5 5.9 %convolution_bitcast_fusion.1 = f32[1,2048,512]{2,1,0:T(8,128)} fusion(bf16[768,2048]{1,0:T(8,128)(2,1)} %bitcast.71, bf16[768,512]{1,0:T(8,128)(2,1)S(1)} %copy-done.8), kind=kOutput, calls=%fused_computation.7 | convolution fusion | flops 1610612736 | bytes 8126464 | tf_op jit(solution)/shard_map/dot_general | solution.py:28
  245.4 3.9 %convolution_bitcast_fusion.2 = f32[1,2048,512]{2,1,0:T(8,128)} fusion(bf16[768,2048]{1,0:T(8,128)(2,1)S(1)} %bitcast.73, bf16[768,512]{1,0:T(8,128)(2,1)S(1)} %copy-done.6), kind=kOutput, calls=%fused_computation.8 | convolution fusion | flops 1610612736 | bytes 8126464 | tf_op jit(solution)/shard_map/dot_general | solution.py:28
  249.4 4.1 %convolution_bitcast_fusion = f32[1,512,2048]{2,1,0:T(8,128)} fusion(bf16[768,2048]{1,0:T(8,128)(2,1)S(1)} %bitcast.75, f32[768,512]{1,0:T(8,128)S(1)} %copy-done.20, f32[768,512]{1,0:T(8,128)S(1)} %copy-done.21), kind=kOutput, calls=%fused_computation.6 | convolution fusion | flops 1614544896 | bytes 10485760 | tf_op jit(solution)/shard_map/dot_general | solution.py:28
  255.0 52.5 %reduce-scatter.2.cloned.1.call-done = f32[256,256]{1,0:T(8,128)} async-done(((f32[2048,256]{1,0:T(8,128)}), f32[256,256]{1,0:T(8,128)}) %reduce-scatter.2.cloned.1.call-update) | async-done | bytes 262160 | tf_op jit(solution)/shard_map/reduce_scatter | solution.py:146
  (80 shorter events, 11.1 us)
Async XLA Ops:
  7.2 92.0 %copy-start = (bf16[1,2048,512]{2,1,0:T(8,128)(2,1)S(1)}, bf16[1,2048,512]{2,1,0:T(8,128)(2,1)}, u32[]{:S(2)}) copy-start(bf16[1,2048,512]{2,1,0:T(8,128)(2,1)} %param.21) | copy-start | bytes 6291460
  7.2 86.3 %all-gather.3.cloned.1.call-start = ((), (), s32[]{:S(2)}) async-start(), calls=%async_computation.5 | async-start | bytes 3932160 | tf_op jit(solution)/shard_map/all_gather | solution.py:110
  19.1 28.7 %copy-start.3 = (bf16[192,2048]{1,0:T(8,128)(2,1)S(1)}, bf16[192,2048]{1,0:T(8,128)(2,1)}, u32[]{:S(2)}) copy-start(bf16[192,2048]{1,0:T(8,128)(2,1)} %param.13) | copy-start | bytes 2359300
  47.7 73.6 %all-gather.5.cloned.1.call-start = ((), (), s32[]{:S(2)}) async-start(), calls=%async_computation.6 | async-start | bytes 3932160 | tf_op jit(solution)/shard_map/all_gather | solution.py:111
  51.0 5.4 %copy-start.16 = (f32[192,2]{0,1:T(2,128)S(1)}, f32[192,2]{0,1:T(2,128)}, u32[]{:S(2)}) copy-start(f32[192,2]{0,1:T(2,128)} %param.15) | copy-start | bytes 4612
  93.5 5.6 %copy-start.17 = (bf16[8,96,2048]{2,1,0:T(8,128)(2,1)S(1)}, bf16[8,96,2048]{2,1,0:T(8,128)(2,1)}, u32[]{:S(2)}) copy-start(bf16[8,96,2048]{2,1,0:T(8,128)(2,1)} %all-gather.3.cloned.1.call-done) | copy-start | bytes 9437188
  127.4 1.9 copy-start.5
  127.4 1.9 copy-start.7
  127.4 2.2 copy-start.2
  172.8 5.7 %copy-start.12 = (bf16[192,256]{1,0:T(8,128)(2,1)S(1)}, bf16[192,256]{1,0:T(8,128)(2,1)}, u32[]{:S(2)}) copy-start(bf16[192,256]{1,0:T(8,128)(2,1)} %param.18) | copy-start | bytes 294916
  172.8 5.7 %copy-start.14 = (bf16[192,256]{1,0:T(8,128)(2,1)S(1)}, bf16[192,256]{1,0:T(8,128)(2,1)}, u32[]{:S(2)}) copy-start(bf16[192,256]{1,0:T(8,128)(2,1)} %param.17) | copy-start | bytes 294916
  172.8 42.3 %all-to-all-start.3 = ((f32[8,96,512]{2,1,0:T(8,128)}), f32[8,96,512]{2,1,0:T(8,128)S(1)}, u32[]{:S(2)}, u32[]{:S(2)}) async-start(f32[8,96,512]{2,1,0:T(8,128)} %bitcast.57), calls=%async_computation.3 | async-start | bytes 3145728 | tf_op jit(solution)/shard_map/all_to_all | solution.py:123
  178.4 129.1 %reduce-scatter.2.cloned.1.call-start = ((), (), s32[]{:S(2)}) async-start(), calls=%async_computation.7 | async-start | bytes 2359296 | tf_op jit(solution)/shard_map/reduce_scatter | solution.py:146
  216.7 11.0 %copy-start.11 = (bf16[192,256]{1,0:T(8,128)(2,1)S(1)}, bf16[192,256]{1,0:T(8,128)(2,1)}, u32[]{:S(2)}) copy-start(bf16[192,256]{1,0:T(8,128)(2,1)} %param.16) | copy-start | bytes 294916
  217.2 10.5 %copy-start.4 = (bf16[2048,256]{1,0:T(8,128)(2,1)S(1)}, bf16[2048,256]{1,0:T(8,128)(2,1)}, u32[]{:S(2)}) copy-start(bf16[2048,256]{1,0:T(8,128)(2,1)} %param.20) | copy-start | bytes 3145732
  219.1 0.7 copy-start.10
  228.8 5.8 %collective-permute-start = (f32[1,512]{1,0:T(1,128)S(1)}, f32[1,512]{1,0:T(1,128)S(1)}, u32[]{:S(2)}, u32[]{:S(2)}) collective-permute-start(f32[1,512]{1,0:T(1,128)S(1)} %get-tuple-element.12), channel_id=1, source_target_pairs={{0,4},{4,8},{8,12},{12,16},{16,20},{20,24},{24,28},{1,5},{5,9},{9,... | collective-permute-start | bytes 6152 | tf_op jit(solution)/shard_map/ppermute | solution.py:18
  232.1 5.5 %collective-permute-start.1 = (f32[1,512]{1,0:T(1,128)S(1)}, f32[1,512]{1,0:T(1,128)S(1)}, u32[]{:S(2)}, u32[]{:S(2)}) collective-permute-start(f32[1,512]{1,0:T(1,128)S(1)} %get-tuple-element.13), channel_id=1, source_target_pairs={{4,0},{8,4},{12,8},{16,12},{20,16},{24,20},{28,24},{5,1},{9,5},{13... | collective-permute-start | bytes 6152 | tf_op jit(solution)/shard_map/ppermute | solution.py:20
  237.6 1.9 copy-start.8
  239.5 5.9 %copy-start.6 = (bf16[768,512]{1,0:T(8,128)(2,1)S(1)}, bf16[768,512]{1,0:T(8,128)(2,1)}, u32[]{:S(2)}) copy-start(bf16[768,512]{1,0:T(8,128)(2,1)} %copy-done.5) | copy-start | bytes 2359300
  239.5 5.9 %copy-start.18 = (bf16[8,96,2048]{2,1,0:T(8,128)(2,1)S(1)}, bf16[8,96,2048]{2,1,0:T(8,128)(2,1)}, u32[]{:S(2)}) copy-start(bf16[8,96,2048]{2,1,0:T(8,128)(2,1)} %all-gather.3.cloned.1.call-done) | copy-start | bytes 9437188
  245.4 3.9 %copy-start.19 = (bf16[8,96,2048]{2,1,0:T(8,128)(2,1)S(1)}, bf16[8,96,2048]{2,1,0:T(8,128)(2,1)}, u32[]{:S(2)}) copy-start(bf16[8,96,2048]{2,1,0:T(8,128)(2,1)} %all-gather.5.cloned.1.call-done) | copy-start | bytes 9437188
  245.4 3.9 %copy-start.20 = (f32[768,512]{1,0:T(8,128)S(1)}, f32[768,512]{1,0:T(8,128)}, u32[]{:S(2)}) copy-start(f32[768,512]{1,0:T(8,128)} %fusion.1) | copy-start | bytes 4718596
  245.4 3.9 %copy-start.21 = (f32[768,512]{1,0:T(8,128)S(1)}, f32[768,512]{1,0:T(8,128)}, u32[]{:S(2)}) copy-start(f32[768,512]{1,0:T(8,128)} %fusion.7) | copy-start | bytes 4718596
  249.4 4.1 %copy-start.13 = (bf16[192,256]{1,0:T(8,128)(2,1)S(1)}, bf16[192,256]{1,0:T(8,128)(2,1)}, u32[]{:S(2)}) copy-start(bf16[192,256]{1,0:T(8,128)(2,1)} %param.18) | copy-start | bytes 294916
  249.4 4.8 %copy-start.9 = (f32[192,256]{1,0:T(8,128)S(1)}, f32[192,256]{1,0:T(8,128)}, u32[]{:S(2)}) copy-start(f32[192,256]{1,0:T(8,128)} %get-tuple-element.20) | copy-start | bytes 589828
  249.4 4.8 %copy-start.15 = (bf16[192,256]{1,0:T(8,128)(2,1)S(1)}, bf16[192,256]{1,0:T(8,128)(2,1)}, u32[]{:S(2)}) copy-start(bf16[192,256]{1,0:T(8,128)(2,1)} %param.17) | copy-start | bytes 294916
  249.4 58.1 %copy-start.1 = (bf16[1,2048,512]{2,1,0:T(8,128)(2,1)S(1)}, bf16[1,2048,512]{2,1,0:T(8,128)(2,1)}, u32[]{:S(2)}) copy-start(bf16[1,2048,512]{2,1,0:T(8,128)(2,1)} %param.21) | copy-start | bytes 6291460
Sparse Core Ops, SparseCore 0:
  47.8 27.5 all-gather.2
  93.6 27.6 all-gather.4
  239.6 67.8 reduce-scatter.1
where the time goes:
time: 315 us; the launch traced here: 314 us
  waiting for transfers between devices  111 us (35%)
  blocking collectives  98.1 us (31%)
  local copies, waits for them, and re-layouts  35.8 us (11%)
  matrix products  35.3 us (11%)
  between operations  14.1 us (4%)
  starting transfers between devices  10.6 us (3%)
  other arithmetic  8.97 us (3%)
    reduce_scatter x1, waiting for transfers between devices, local(): lax.psum_scatter(contract_rows(residual, mixed_act), 'sp', scatter_dimens...  52.5 us
    all_to_all x1, blocking collectives, local(): lax.all_to_all(grouped, 'tp', split_axis=1, concat_axis=1, tiled=True)  39.4 us
    all_to_all x1, waiting for transfers between devices, local(): lax.all_to_all(shares, 'sp', split_axis=0, concat_axis=0, tiled=True)  36.5 us
    all_to_all x1, blocking collectives, local(): lax.all_to_all(sliced[0], 'sp', split_axis=0, concat_axis=0, tiled=True)  27.3 us
    all_to_all x1, blocking collectives, local(): lax.all_to_all(sliced[1], 'sp', split_axis=0, concat_axis=0, tiled=True)  23.4 us
    all_gather x1, waiting for transfers between devices, local(): lax.all_gather(arrived[1], 'tp', axis=2, tiled=True)  19.1 us
    dot_general x4, matrix products, contract_rows(): lax.dot_general(left, right, (((0,), (0,)), ((), ())), preferred_element_...  15.8 us
    dot_general x3, matrix products, contract_cols(): lax.dot_general(left, right, (((1,), (1,)), ((), ())), preferred_element_...  9.8 us
  transfers between devices with their start and end apart: 6, of which 4 were waited for; matrix products, arithmetic and copies ran while one was open for 15% of the time, Pallas kernels for 0%

commit v1 on v0

--- a/solution.py
+++ b/solution.py
@@ -118,7 +118,10 @@
         down_proj[0],
     )
     grouped = partial_value.reshape(expert_count * capacity, tp_count, part_width)
-    pieces = lax.all_to_all(grouped, "tp", split_axis=1, concat_axis=1, tiled=True)
+    pieces = jnp.concatenate(
+        lax.all_to_all(jnp.stack(jnp.split(grouped, lax.axis_size("tp"), axis=1)), "tp", 0, 0),
+        axis=1,
+    )
     shares = jnp.sum(pieces.astype(jnp.float32), axis=1).reshape(expert_count, capacity, part_width)
     returned = lax.all_to_all(shares, "sp", split_axis=0, concat_axis=0, tiled=True)
     picked = returned.reshape(-1, part_width)[slot_index]

time: 315 us -> 334 us (1.060)
  local copies, waits for them, and re-layouts: 35.8 us -> 53.1 us
    split x0 -> x1, local copies, waits for them, and re-layouts: none -> 10.7 us  [local(): jnp.split(grouped, lax.axis_size('tp'), axis=1)]
    reshape x1, local copies, waits for them, and re-layouts: 0.29 us -> 6.15 us  [local(): partial_value.reshape(expert_count * capacity, tp_count, part_width)]
  transfers between devices with their start and end apart: 6 -> 6, of which waited for: 4 -> 4; matrix products, arithmetic and copies ran while one was open for 15% -> 14% of each run, Pallas kernels for 0% -> 0%
where the time goes in v1:
time: 334 us
  waiting for transfers between devices  111 us (33%)
  blocking collectives  98.1 us (29%)
  local copies, waits for them, and re-layouts  53.1 us (16%)
  matrix products  36.9 us (11%)
  between operations  14.2 us (4%)
  starting transfers between devices  10.4 us (3%)
  other arithmetic  9.41 us (3%)
    reduce_scatter x1, waiting for transfers between devices, local(): lax.psum_scatter(contract_rows(residual, mixed_act), 'sp', scatter_dimens...  52.5 us
    all_to_all x1, blocking collectives, local(): lax.all_to_all(jnp.stack(jnp.split(grouped, lax.axis_size('tp'), axis=1))...  39.4 us
    all_to_all x1, waiting for transfers between devices, local(): lax.all_to_all(shares, 'sp', split_axis=0, concat_axis=0, tiled=True)  36.5 us
    all_to_all x1, blocking collectives, local(): lax.all_to_all(sliced[0], 'sp', split_axis=0, concat_axis=0, tiled=True)  27.3 us
    all_to_all x1, blocking collectives, local(): lax.all_to_all(sliced[1], 'sp', split_axis=0, concat_axis=0, tiled=True)  23.4 us
    all_gather x1, waiting for transfers between devices, local(): lax.all_gather(arrived[1], 'tp', axis=2, tiled=True)  19.1 us
    dot_general x4, matrix products, contract_rows(): lax.dot_general(left, right, (((0,), (0,)), ((), ())), preferred_element_...  15.8 us
    dot_general x3, matrix products, contract_cols(): lax.dot_general(left, right, (((1,), (1,)), ((), ())), preferred_element_...  11.5 us
  transfers between devices with their start and end apart: 6, of which 4 were waited for; matrix products, arithmetic and copies ran while one was open for 14% of the time, Pallas kernels for 0%

profile of v1, /device:TPU:0, one launch (start us, length us, event | category | flops | bytes accessed | tf_op | source)
XLA Modules:
  0.0 333.6 jit_solution(2592326290990164199)
XLA Ops:
  10.7 2.9 scatter_custom_fusion
  14.8 4.2 %gather_fusion = bf16[768,2048]{1,0:T(8,128)(2,1)} fusion(bf16[193,2048]{1,0:T(8,128)(2,1)S(1)} %concatenate.18, s32[1024]{0:T(1024)S(1)} %get-tuple-element.26), kind=kCustom, calls=%fused_computation | custom fusion | bytes 6294528 | tf_op jit(solution)/shard_map/gather | solution.py:94
  19.1 1.3 constant_dynamic-slice_fusion.2
  20.3 27.3 %all_to_all.20 = bf16[8,96,512]{2,1,0:T(8,128)(2,1)} all-to-all(bf16[8,96,512]{2,1,0:T(8,128)(2,1)S(1)} %constant_dynamic-slice_fusion.2), channel_id=1, replica_groups=mesh['sp'=8,'tp'=4] {'sp'}, dimensions={0} | all-to-all | bytes 1572864 | tf_op jit(solution)/shard_map/all_to_all | solution.py:106
  47.7 3.3 mul.141
  51.0 5.4 %mul.142 = f32[384,2048]{1,0:T(8,128)} reshape(f32[192,2,2048]{2,1,0:T(2,128)} %mul.141) | data formatting | bytes 6291456 | tf_op jit(solution)/shard_map/mul | solution.py:95
  56.7 2.1 multiply_convert_fusion
  58.8 1.3 concatenate.19
  60.1 8.7 %gather_fusion.1 = bf16[768,2048]{1,0:T(8,128)(2,1)} fusion(bf16[385,2048]{1,0:T(8,128)(2,1)} %concatenate.19, s32[1024]{0:T(1024)S(1)} %get-tuple-element.25), kind=kCustom, calls=%fused_computation.1 | custom fusion | bytes 6294528 | tf_op jit(solution)/shard_map/gather | solution.py:98
  70.0 23.4 %all_to_all.21 = bf16[8,96,512]{2,1,0:T(8,128)(2,1)} all-to-all(bf16[8,96,512]{2,1,0:T(8,128)(2,1)S(1)} %constant_dynamic-slice_fusion.1), channel_id=1, replica_groups=mesh['sp'=8,'tp'=4] {'sp'}, dimensions={0} | all-to-all | bytes 1572864 | tf_op jit(solution)/shard_map/all_to_all | solution.py:107
  93.5 5.7 %fusion.1 = f32[768,512]{1,0:T(8,128)} fusion(bf16[768,2048]{1,0:T(8,128)(2,1)} %bitcast.80, bf16[1,2048,512]{2,1,0:T(8,128)(2,1)} %param.22), kind=kOutput, calls=%fused_computation.12 | convolution fusion | flops 1610612736 | bytes 6815744 | tf_op jit(solution)/shard_map/dot_general | solution.py:41
  99.2 3.0 fusion.7
  102.2 19.1 %all-gather.5.cloned.1.call-done = bf16[8,96,2048]{2,1,0:T(8,128)(2,1)} async-done(((bf16[8,96,512]{2,1,0:T(8,128)(2,1)}), bf16[8,96,2048]{2,1,0:T(8,128)(2,1)}) %all-gather.5.cloned.1.call-update) | async-done | bytes 3145744 | tf_op jit(solution)/shard_map/all_gather | solution.py:111
  121.2 6.1 %select_convert_fusion = (bf16[768,512]{1,0:T(8,128)(2,1)S(1)}, bf16[768,512]{1,0:T(8,128)(2,1)S(1)}) fusion(f32[768,512]{1,0:T(8,128)} %fusion.1, f32[768,512]{1,0:T(8,128)} %fusion.7, bf16[768,2048]{1,0:T(8,128)(2,1)} %bitcast.84, bf16[1,512,2048]{2,1,0:T(8,128)(2,1)} %param.23), kind=kOutput, calls=%fused_computation.21 | convolution fusion | flops 1619263488 | bytes 9961472 | tf_op jit(solution)/shard_map/dot_general | solution.py:34
  127.4 1.8 fusion.5
  129.6 3.5 %add_convert_fusion = bf16[768,2048]{1,0:T(8,128)(2,1)} fusion(f32[768,2048]{1,0:T(8,128)S(1)} %fusion.5, bf16[768,512]{1,0:T(8,128)(2,1)S(1)} %get-tuple-element.8, bf16[1,2048,512]{2,1,0:T(8,128)(2,1)S(1)} %copy-done.2), kind=kOutput, calls=%fused_computation.5 | convolution fusion | flops 1613758464 | bytes 12320768 | tf_op jit(solution)/shard_map/dot_general | solution.py:34
  133.1 6.1 %reshape.102 = bf16[768,4,512]{2,1,0:T(4,128)(2,1)} reshape(bf16[768,2048]{1,0:T(8,128)(2,1)} %add_convert_fusion) | data formatting | bytes 6291456 | tf_op jit(solution)/shard_map/reshape | solution.py:120
  139.2 10.7 %fusion.34 = (bf16[768,1,512]{2,1,0:T(2,128)(2,1)S(1)}, bf16[768,1,512]{2,1,0:T(2,128)(2,1)S(1)}, bf16[768,1,512]{2,1,0:T(2,128)(2,1)S(1)}, bf16[768,1,512]{2,1,0:T(2,128)(2,1)S(1)}) fusion(bf16[768,4,512]{2,1,0:T(4,128)(2,1)} %reshape.102), kind=kLoop, calls=%fused_computation.88 | loop fusion | bytes 6291456 | tf_op jit(solution)/shard_map/split | solution.py:122
  151.2 39.4 %all_to_all.22 = bf16[4,768,1,512]{3,1,2,0:T(8,128)(2,1)S(1)} all-to-all(bf16[4,768,1,512]{3,1,2,0:T(8,128)(2,1)S(1)} %pad_maximum_fusion), channel_id=1, replica_groups=mesh['sp'=8,'tp'=4] {'tp'}, dimensions={0} | all-to-all | bytes 6291456 | tf_op jit(solution)/shard_map/all_to_all | solution.py:122
  190.6 1.6 convert_reduce_fusion
  192.3 5.6 %all-to-all-start.3 = ((f32[8,96,512]{2,1,0:T(8,128)}), f32[8,96,512]{2,1,0:T(8,128)S(1)}, u32[]{:S(2)}, u32[]{:S(2)}) async-start(f32[8,96,512]{2,1,0:T(8,128)} %bitcast.63), calls=%async_computation.3 | async-start | bytes 3145728 | tf_op jit(solution)/shard_map/all_to_all | solution.py:126
  198.0 36.5 %all-to-all-done.3 = f32[8,96,512]{2,1,0:T(8,128)S(1)} async-done(((f32[8,96,512]{2,1,0:T(8,128)}), f32[8,96,512]{2,1,0:T(8,128)S(1)}, u32[]{:S(2)}, u32[]{:S(2)}) %all-to-all-start.3) | async-done | bytes 1572896 | tf_op jit(solution)/shard_map/all_to_all | solution.py:126
  234.6 1.6 gather_fusion.2
  239.3 7.9 %all_gather.11 = bf16[192,2048]{1,0:T(8,128)(2,1)S(1)} all-gather(bf16[192,512]{1,0:T(8,128)(2,1)S(1)} %add_convert_fusion.1), channel_id=1, replica_groups=mesh['sp'=8,'tp'=4] {'tp'}, dimensions={1}, use_global_device_ids=true | all-gather | bytes 983040 | tf_op jit(solution)/shard_map/all_gather | solution.py:131
  248.2 3.3 %collective-permute-start = (f32[1,512]{1,0:T(1,128)S(1)}, f32[1,512]{1,0:T(1,128)S(1)}, u32[]{:S(2)}, u32[]{:S(2)}) collective-permute-start(f32[1,512]{1,0:T(1,128)S(1)} %get-tuple-element.16), channel_id=1, source_target_pairs={{0,4},{4,8},{8,12},{12,16},{16,20},{20,24},{24,28},{1,5},{5,9},{9,... | collective-permute-start | bytes 6152 | tf_op jit(solution)/shard_map/ppermute | solution.py:18
  251.6 1.3 collective-permute-start.1
  253.8 3.3 collective-permute-done.1
  257.1 1.9 fusion.21
  259.0 5.9 %convolution_bitcast_fusion.1 = f32[1,2048,512]{2,1,0:T(8,128)} fusion(bf16[768,2048]{1,0:T(8,128)(2,1)} %bitcast.81, bf16[768,512]{1,0:T(8,128)(2,1)S(1)} %copy-done.8), kind=kOutput, calls=%fused_computation.7 | convolution fusion | flops 1610612736 | bytes 8126464 | tf_op jit(solution)/shard_map/dot_general | solution.py:28
  264.9 3.9 %convolution_bitcast_fusion.2 = f32[1,2048,512]{2,1,0:T(8,128)} fusion(bf16[768,2048]{1,0:T(8,128)(2,1)S(1)} %bitcast.83, bf16[768,512]{1,0:T(8,128)(2,1)S(1)} %copy-done.6), kind=kOutput, calls=%fused_computation.8 | convolution fusion | flops 1610612736 | bytes 8126464 | tf_op jit(solution)/shard_map/dot_general | solution.py:28
  268.9 4.1 %convolution_bitcast_fusion = f32[1,512,2048]{2,1,0:T(8,128)} fusion(bf16[768,2048]{1,0:T(8,128)(2,1)S(1)} %bitcast.85, f32[768,512]{1,0:T(8,128)S(1)} %copy-done.20, f32[768,512]{1,0:T(8,128)S(1)} %copy-done.21), kind=kOutput, calls=%fused_computation.6 | convolution fusion | flops 1614544896 | bytes 10485760 | tf_op jit(solution)/shard_map/dot_general | solution.py:28
  274.5 52.5 %reduce-scatter.2.cloned.1.call-done = f32[256,256]{1,0:T(8,128)} async-done(((f32[2048,256]{1,0:T(8,128)}), f32[256,256]{1,0:T(8,128)}) %reduce-scatter.2.cloned.1.call-update) | async-done | bytes 262160 | tf_op jit(solution)/shard_map/reduce_scatter | solution.py:149
  (86 shorter events, 14.5 us)
Async XLA Ops:
  7.2 92.0 %copy-start = (bf16[1,2048,512]{2,1,0:T(8,128)(2,1)S(1)}, bf16[1,2048,512]{2,1,0:T(8,128)(2,1)}, u32[]{:S(2)}) copy-start(bf16[1,2048,512]{2,1,0:T(8,128)(2,1)} %param.21) | copy-start | bytes 6291460
  7.2 86.3 %all-gather.3.cloned.1.call-start = ((), (), s32[]{:S(2)}) async-start(), calls=%async_computation.5 | async-start | bytes 3932160 | tf_op jit(solution)/shard_map/all_gather | solution.py:110
  19.1 28.7 %copy-start.3 = (bf16[192,2048]{1,0:T(8,128)(2,1)S(1)}, bf16[192,2048]{1,0:T(8,128)(2,1)}, u32[]{:S(2)}) copy-start(bf16[192,2048]{1,0:T(8,128)(2,1)} %param.13) | copy-start | bytes 2359300
  47.7 73.6 %all-gather.5.cloned.1.call-start = ((), (), s32[]{:S(2)}) async-start(), calls=%async_computation.6 | async-start | bytes 3932160 | tf_op jit(solution)/shard_map/all_gather | solution.py:111
  51.0 5.4 %copy-start.16 = (f32[192,2]{0,1:T(2,128)S(1)}, f32[192,2]{0,1:T(2,128)}, u32[]{:S(2)}) copy-start(f32[192,2]{0,1:T(2,128)} %param.15) | copy-start | bytes 4612
  93.5 5.7 %copy-start.17 = (bf16[8,96,2048]{2,1,0:T(8,128)(2,1)S(1)}, bf16[8,96,2048]{2,1,0:T(8,128)(2,1)}, u32[]{:S(2)}) copy-start(bf16[8,96,2048]{2,1,0:T(8,128)(2,1)} %all-gather.3.cloned.1.call-done) | copy-start | bytes 9437188
  127.4 1.9 copy-start.5
  127.4 1.9 copy-start.7
  127.4 2.2 copy-start.2
  192.3 5.7 %copy-start.12 = (bf16[192,256]{1,0:T(8,128)(2,1)S(1)}, bf16[192,256]{1,0:T(8,128)(2,1)}, u32[]{:S(2)}) copy-start(bf16[192,256]{1,0:T(8,128)(2,1)} %param.18) | copy-start | bytes 294916
  192.3 5.7 %copy-start.14 = (bf16[192,256]{1,0:T(8,128)(2,1)S(1)}, bf16[192,256]{1,0:T(8,128)(2,1)}, u32[]{:S(2)}) copy-start(bf16[192,256]{1,0:T(8,128)(2,1)} %param.17) | copy-start | bytes 294916
  192.3 42.3 %all-to-all-start.3 = ((f32[8,96,512]{2,1,0:T(8,128)}), f32[8,96,512]{2,1,0:T(8,128)S(1)}, u32[]{:S(2)}, u32[]{:S(2)}) async-start(f32[8,96,512]{2,1,0:T(8,128)} %bitcast.63), calls=%async_computation.3 | async-start | bytes 3145728 | tf_op jit(solution)/shard_map/all_to_all | solution.py:126
  197.9 129.1 %reduce-scatter.2.cloned.1.call-start = ((), (), s32[]{:S(2)}) async-start(), calls=%async_computation.7 | async-start | bytes 2359296 | tf_op jit(solution)/shard_map/reduce_scatter | solution.py:149
  236.2 11.0 %copy-start.11 = (bf16[192,256]{1,0:T(8,128)(2,1)S(1)}, bf16[192,256]{1,0:T(8,128)(2,1)}, u32[]{:S(2)}) copy-start(bf16[192,256]{1,0:T(8,128)(2,1)} %param.16) | copy-start | bytes 294916
  236.7 10.5 %copy-start.4 = (bf16[2048,256]{1,0:T(8,128)(2,1)S(1)}, bf16[2048,256]{1,0:T(8,128)(2,1)}, u32[]{:S(2)}) copy-start(bf16[2048,256]{1,0:T(8,128)(2,1)} %param.20) | copy-start | bytes 3145732
  238.6 0.7 copy-start.10
  248.2 5.5 %collective-permute-start = (f32[1,512]{1,0:T(1,128)S(1)}, f32[1,512]{1,0:T(1,128)S(1)}, u32[]{:S(2)}, u32[]{:S(2)}) collective-permute-start(f32[1,512]{1,0:T(1,128)S(1)} %get-tuple-element.16), channel_id=1, source_target_pairs={{0,4},{4,8},{8,12},{12,16},{16,20},{20,24},{24,28},{1,5},{5,9},{9,... | collective-permute-start | bytes 6152 | tf_op jit(solution)/shard_map/ppermute | solution.py:18
  251.6 5.5 %collective-permute-start.1 = (f32[1,512]{1,0:T(1,128)S(1)}, f32[1,512]{1,0:T(1,128)S(1)}, u32[]{:S(2)}, u32[]{:S(2)}) collective-permute-start(f32[1,512]{1,0:T(1,128)S(1)} %get-tuple-element.17), channel_id=1, source_target_pairs={{4,0},{8,4},{12,8},{16,12},{20,16},{24,20},{28,24},{5,1},{9,5},{13... | collective-permute-start | bytes 6152 | tf_op jit(solution)/shard_map/ppermute | solution.py:20
  257.1 1.9 copy-start.8
  259.0 5.9 %copy-start.6 = (bf16[768,512]{1,0:T(8,128)(2,1)S(1)}, bf16[768,512]{1,0:T(8,128)(2,1)}, u32[]{:S(2)}) copy-start(bf16[768,512]{1,0:T(8,128)(2,1)} %copy-done.5) | copy-start | bytes 2359300
  259.0 5.9 %copy-start.18 = (bf16[8,96,2048]{2,1,0:T(8,128)(2,1)S(1)}, bf16[8,96,2048]{2,1,0:T(8,128)(2,1)}, u32[]{:S(2)}) copy-start(bf16[8,96,2048]{2,1,0:T(8,128)(2,1)} %all-gather.3.cloned.1.call-done) | copy-start | bytes 9437188
  264.9 3.9 %copy-start.19 = (bf16[8,96,2048]{2,1,0:T(8,128)(2,1)S(1)}, bf16[8,96,2048]{2,1,0:T(8,128)(2,1)}, u32[]{:S(2)}) copy-start(bf16[8,96,2048]{2,1,0:T(8,128)(2,1)} %all-gather.5.cloned.1.call-done) | copy-start | bytes 9437188
  264.9 3.9 %copy-start.20 = (f32[768,512]{1,0:T(8,128)S(1)}, f32[768,512]{1,0:T(8,128)}, u32[]{:S(2)}) copy-start(f32[768,512]{1,0:T(8,128)} %fusion.1) | copy-start | bytes 4718596
  264.9 3.9 %copy-start.21 = (f32[768,512]{1,0:T(8,128)S(1)}, f32[768,512]{1,0:T(8,128)}, u32[]{:S(2)}) copy-start(f32[768,512]{1,0:T(8,128)} %fusion.7) | copy-start | bytes 4718596
  268.9 4.1 %copy-start.13 = (bf16[192,256]{1,0:T(8,128)(2,1)S(1)}, bf16[192,256]{1,0:T(8,128)(2,1)}, u32[]{:S(2)}) copy-start(bf16[192,256]{1,0:T(8,128)(2,1)} %param.18) | copy-start | bytes 294916
  268.9 4.8 %copy-start.9 = (f32[192,256]{1,0:T(8,128)S(1)}, f32[192,256]{1,0:T(8,128)}, u32[]{:S(2)}) copy-start(f32[192,256]{1,0:T(8,128)} %get-tuple-element.24) | copy-start | bytes 589828
  268.9 4.8 %copy-start.15 = (bf16[192,256]{1,0:T(8,128)(2,1)S(1)}, bf16[192,256]{1,0:T(8,128)(2,1)}, u32[]{:S(2)}) copy-start(bf16[192,256]{1,0:T(8,128)(2,1)} %param.17) | copy-start | bytes 294916
  268.9 58.2 %copy-start.1 = (bf16[1,2048,512]{2,1,0:T(8,128)(2,1)S(1)}, bf16[1,2048,512]{2,1,0:T(8,128)(2,1)}, u32[]{:S(2)}) copy-start(bf16[1,2048,512]{2,1,0:T(8,128)(2,1)} %param.21) | copy-start | bytes 6291460
Sparse Core Ops, SparseCore 0:
  47.8 27.5 all-gather.2
  93.6 27.6 all-gather.4
  259.1 67.8 reduce-scatter.1
